TPU v7x, 32 devices: a whole 2x2x4 slice. The times are simulated.
32 devices in a mesh: grp: 2 (over y), sp: 4 (over z), tp: 4 (over x, core).
Axes of the slice: x: 2, y: 2, z: 4, core: 2. Of those that a mesh axis runs over, the one named last changes fastest.
Arguments:
- hidden_in: bfloat16 [5120, 4096], P(('grp', 'sp'), 'tp'), parts along dimension 0, may hold values from -64 to 64
- norm_gain: float32 [2, 4096], replicated, may hold values from 0.1 to 1.9
- w_pool_in: bfloat16 [2, 4096, 1024], P(None, 'sp', 'tp'), may hold values from -0.09375 to 0.09375
- w_pool_gate: bfloat16 [2, 4096, 1024], P(None, 'sp', 'tp'), may hold values from -0.09375 to 0.09375
- group_mix: bfloat16 [2, 16, 64, 64], replicated, may hold values from -0.75 to 0.75
- w_out: bfloat16 [2, 1024, 4096], P(None, 'sp', 'tp'), may hold values from -0.1875 to 0.1875
Outputs:
- hidden_out: bfloat16 [5120, 4096], P(('grp', 'sp'), 'tp'), parts along dimension 0
There are 2 independent parts, one for each index of `grp`. A program takes and returns all parts, laid end to end along the dimension named above; an argument that names none is the same for every part. Nothing has to cross between parts.
All inputs are finite; a program needn't handle non-finite values.
Results may differ from a plain program's by a relative error of at most 0.012.
Values may be sent and summed in bfloat16 or wider, within the bound.
A program may use at most 64 MiB of HBM per device.

v0:
```python
import jax
import jax.numpy as jnp
from jax import lax
from jax.sharding import PartitionSpec as P

GROUP = 64


norm_eps = 1e-06


def with_halo(array, sides, width):
    for axis, dim in sides:
        size, length = (lax.axis_size(axis), array.shape[dim])
        up = [(i, (i + 1) % size) for i in range(size - 1)]
        down = [(j, i) for i, j in up]
        last = lax.slice_in_dim(array, length - width, length, axis=dim)
        leading = lax.slice_in_dim(array, 0, width, axis=dim)
        before = lax.ppermute(last, axis, up)
        after = lax.ppermute(leading, axis, down)
        array = jnp.concatenate([before, array, after], axis=dim)
    return array


def local(hidden_in, norm_gain, w_pool_in, w_pool_gate, group_mix, w_out):
    tok_rows = hidden_in.shape[0]
    col_count = hidden_in.shape[1]
    chan_count = w_pool_in.shape[2]
    group_local = chan_count // GROUP
    layer_count = w_pool_in.shape[0]
    col_rank = lax.axis_index("tp")
    row_rank = lax.axis_index("sp")
    total_rows = tok_rows * lax.axis_size("sp")
    full_width = col_count * lax.axis_size("tp")
    position = row_rank * tok_rows + jnp.arange(tok_rows, dtype=jnp.int32)
    channel_code = (col_rank * group_local + jnp.arange(chan_count, dtype=jnp.int32) // GROUP) % 4
    every_in, every_gate, every_out = (
        lax.all_gather(w_pool_in, "sp", axis=1, tiled=True),
        lax.all_gather(w_pool_gate, "sp", axis=1, tiled=True),
        lax.all_gather(w_out, "sp", axis=1, tiled=True),
    )
    resid = hidden_in
    for layer in range(layer_count):
        weight_in = every_in[layer]
        weight_gate = every_gate[layer]
        weight_out = every_out[layer]
        resid_f = resid.astype(jnp.float32)
        squares = lax.psum(jnp.sum(resid_f * resid_f, axis=1), "tp")
        scaling = lax.rsqrt(squares / full_width + norm_eps)
        own_gain = lax.dynamic_slice_in_dim(norm_gain[layer], col_rank * col_count, col_count)
        normed = (resid_f * scaling[:, None] * own_gain[None, :]).astype(jnp.bfloat16)
        piece = lax.all_gather(normed, "tp", axis=1, tiled=True)
        pool_sum = jnp.dot(piece, weight_in, preferred_element_type=jnp.float32)
        gate_sum = jnp.dot(piece, weight_gate, preferred_element_type=jnp.float32)
        pool_in = pool_sum.astype(jnp.bfloat16)
        gate = gate_sum.astype(jnp.bfloat16)
        padded = with_halo(pool_in, (("sp", 0),), 8).astype(jnp.float32)
        running = jnp.zeros((tok_rows, chan_count), jnp.float32)
        averaged = jnp.zeros((tok_rows, chan_count), jnp.float32)
        previous = 0
        for code_value, half in enumerate((1, 2, 4, 8)):
            for offset in list(range(-half, -previous)) + list(range(previous, half)):
                running = running + padded[8 + offset : 8 + offset + tok_rows]
            previous = half
            counted = (
                jnp.minimum(position + half, total_rows) - jnp.maximum(position - half, 0)
            ).astype(jnp.float32)
            averaged = jnp.where(
                channel_code[None, :] == code_value, running / counted[:, None], averaged
            )
        pooled = (averaged - padded[8 : 8 + tok_rows]).astype(jnp.bfloat16)
        own_mix = lax.dynamic_slice_in_dim(group_mix[layer], col_rank * group_local, group_local, 0)
        mixed = jnp.einsum(
            "tgc,gcd->tgd",
            pooled.reshape(tok_rows, group_local, GROUP),
            own_mix,
            preferred_element_type=jnp.float32,
        ).reshape(tok_rows, chan_count)
        branch = (mixed * jax.nn.silu(gate.astype(jnp.float32))).astype(jnp.bfloat16)
        projected = jnp.dot(
            lax.all_gather(branch, "tp", axis=1, tiled=True),
            weight_out,
            preferred_element_type=jnp.float32,
        )
        resid = (resid_f + projected).astype(jnp.bfloat16)
    return resid


def solution(mesh):
    in_specs = (
        P(("grp", "sp"), "tp"),
        P(),
        P(None, "sp", "tp"),
        P(None, "sp", "tp"),
        P(),
        P(None, "sp", "tp"),
    )
    out_specs = P(("grp", "sp"), "tp")
    return jax.shard_map(local, mesh=mesh, in_specs=in_specs, out_specs=out_specs, check_vma=False)
```

profile of v0, /device:TPU:0, one launch (start us, length us, event | category | flops | bytes accessed | tf_op | source)
XLA Modules:
  0.0 417.1 jit_solution(7042506414387707074)
XLA Ops:
  6.5 0.7 all-gather.10.cloned.1.call-update
  7.3 1.6 fusion
  9.0 8.4 %psum.14 = f32[640]{0:T(1024)S(1)} all-reduce(f32[640]{0:T(1024)S(1)} %fusion), channel_id=1, replica_groups=mesh['grp'=2,'sp'=4,'tp'=4] {'tp'}, use_global_device_ids=true, to_apply=%region_1.2 | all-reduce | flops 640 | bytes 5120 | tf_op jit(solution)/shard_map/psum | solution.py:48
  17.3 0.9 fusion.41
  18.2 1.4 fusion.2
  19.7 0.7 all-gather.12.cloned.1.call-update
  20.5 0.5 all-gather.16.cloned.1.call-update
  21.2 71.2 %all-gather.10.cloned.1.call-done = bf16[2,4096,256]{2,1,0:T(8,128)(2,1)} async-done(((bf16[2,1024,256]{2,1,0:T(8,128)(2,1)}), bf16[2,4096,256]{2,1,0:T(8,128)(2,1)}) %all-gather.10.cloned.1.call-update) | async-done | bytes 4194320 | tf_op jit(solution)/shard_map/all_gather | solution.py:38
  92.4 40.5 %all-gather.8.cloned.1.call-done = bf16[640,4096]{1,0:T(8,128)(2,1)} async-done(((bf16[640,1024]{1,0:T(8,128)(2,1)}), bf16[640,4096]{1,0:T(8,128)(2,1)}) %all-gather.8.cloned.1.call-update) | async-done | bytes 5242896 | tf_op jit(solution)/shard_map/all_gather | solution.py:52
  132.9 4.7 %fusion.14 = bf16[640,256]{1,0:T(8,128)(2,1)S(1)} fusion(bf16[640,4096]{1,0:T(8,128)(2,1)} %all-gather.8.cloned.1.call-done, bf16[2,4096,256]{2,1,0:T(8,128)(2,1)} %all-gather.10.cloned.1.call-done), kind=kOutput, calls=%fused_computation.26 | convolution fusion | flops 1342341120 | bytes 7667712 | tf_op jit(solution)/shard_map/dot_general | solution.py:53
  137.6 3.4 collective-permute-start
  141.0 1.3 collective-permute-start.1
  142.3 4.2 %collective-permute-done.1 = bf16[8,256]{1,0:T(8,128)(2,1)S(1)} collective-permute-done((bf16[8,256]{1,0:T(8,128)(2,1)S(1)}, bf16[8,256]{1,0:T(8,128)(2,1)S(1)}, u32[]{:S(2)}, u32[]{:S(2)}) %collective-permute-start.1) | collective-permute-done | bytes 4128 | tf_op jit(solution)/shard_map/ppermute | solution.py:20
  146.5 1.5 fusion.26
  148.2 0.3 fusion.30
  148.7 66.5 %all-gather.12.cloned.1.call-done = bf16[2,4096,256]{2,1,0:T(8,128)(2,1)} async-done(((bf16[2,1024,256]{2,1,0:T(8,128)(2,1)}), bf16[2,4096,256]{2,1,0:T(8,128)(2,1)}) %all-gather.12.cloned.1.call-update) | async-done | bytes 4194320 | tf_op jit(solution)/shard_map/all_gather | solution.py:39
  215.3 5.4 %multiply_convert_fusion.1 = bf16[640,256]{1,0:T(8,128)(2,1)} fusion(f32[640,256]{1,0:T(8,128)S(1)} %copy.15, bf16[640,4096]{1,0:T(8,128)(2,1)} %all-gather.8.cloned.1.call-done, bf16[2,4096,256]{2,1,0:T(8,128)(2,1)} %all-gather.12.cloned.1.call-done), kind=kOutput, calls=%fused_computation.69 | convolution fusion | flops 1343488000 | bytes 8323072 | tf_op jit(solution)/shard_map/dot_general | solution.py:54
  220.8 75.1 %all-gather.16.cloned.1.call-done = bf16[2,1024,1024]{2,1,0:T(8,128)(2,1)} async-done(((bf16[2,256,1024]{2,1,0:T(8,128)(2,1)}), bf16[2,1024,1024]{2,1,0:T(8,128)(2,1)}) %all-gather.16.cloned.1.call-update) | async-done | bytes 4194320 | tf_op jit(solution)/shard_map/all_gather | solution.py:40
  295.9 18.2 %all-gather.14.cloned.1.call-done = bf16[640,1024]{1,0:T(8,128)(2,1)} async-done(((bf16[640,256]{1,0:T(8,128)(2,1)}), bf16[640,1024]{1,0:T(8,128)(2,1)}) %all-gather.14.cloned.1.call-update) | async-done | bytes 1310736 | tf_op jit(solution)/shard_map/all_gather | solution.py:81
  314.1 3.7 fusion.4
  317.8 5.9 %psum.15 = f32[640]{0:T(1024)S(1)} all-reduce(f32[640]{0:T(1024)S(1)} %get-tuple-element.13), channel_id=1, replica_groups=mesh['grp'=2,'sp'=4,'tp'=4] {'tp'}, use_global_device_ids=true, to_apply=%region_3.4 | all-reduce | flops 640 | bytes 5120 | tf_op jit(solution)/shard_map/psum | solution.py:48
  323.7 1.4 fusion.6
  325.2 41.6 %all-gather.18.cloned.1.call-done = bf16[640,4096]{1,0:T(8,128)(2,1)} async-done(((bf16[640,1024]{1,0:T(8,128)(2,1)}), bf16[640,4096]{1,0:T(8,128)(2,1)}) %all-gather.18.cloned.1.call-update) | async-done | bytes 5242896 | tf_op jit(solution)/shard_map/all_gather | solution.py:52
  366.8 4.7 %fusion.17 = bf16[640,256]{1,0:T(8,128)(2,1)S(1)} fusion(bf16[640,4096]{1,0:T(8,128)(2,1)} %all-gather.18.cloned.1.call-done, bf16[2,4096,256]{2,1,0:T(8,128)(2,1)} %all-gather.10.cloned.1.call-done), kind=kOutput, calls=%fused_computation.29 | convolution fusion | flops 1342341120 | bytes 7667712 | tf_op jit(solution)/shard_map/dot_general | solution.py:53
  371.5 3.4 collective-permute-start.2
  374.9 1.5 collective-permute-start.3
  376.4 4.0 collective-permute-done.3
  380.5 1.5 fusion.27
  382.1 0.3 fusion.28
  382.7 5.4 %multiply_convert_fusion = bf16[640,256]{1,0:T(8,128)(2,1)} fusion(f32[640,256]{1,0:T(8,128)S(1)} %copy.18, bf16[640,4096]{1,0:T(8,128)(2,1)} %all-gather.18.cloned.1.call-done, bf16[2,4096,256]{2,1,0:T(8,128)(2,1)} %all-gather.12.cloned.1.call-done), kind=kOutput, calls=%fused_computation.68 | convolution fusion | flops 1343488000 | bytes 8323072 | tf_op jit(solution)/shard_map/dot_general | solution.py:54
  388.1 17.6 %all-gather.20.cloned.1.call-done = bf16[640,1024]{1,0:T(8,128)(2,1)} async-done(((bf16[640,256]{1,0:T(8,128)(2,1)}), bf16[640,1024]{1,0:T(8,128)(2,1)}) %all-gather.20.cloned.1.call-update) | async-done | bytes 1310736 | tf_op jit(solution)/shard_map/all_gather | solution.py:81
  405.7 4.6 %fusion.7 = bf16[640,1024]{1,0:T(8,128)(2,1)} fusion(bf16[640,1024]{1,0:T(8,128)(2,1)S(1)} %get-tuple-element.14, bf16[640,1024]{1,0:T(8,128)(2,1)} %all-gather.20.cloned.1.call-done, bf16[2,1024,1024]{2,1,0:T(8,128)(2,1)} %all-gather.16.cloned.1.call-done), kind=kOutput, calls=%fused_computation.13 | convolution fusion | flops 1344143360 | bytes 6029312 | tf_op jit(solution)/shard_map/dot_general | solution.py:80
  (34 shorter events, 1.4 us)
Async XLA Ops:
  6.5 11.7 %copy-start = (bf16[640,1024]{1,0:T(8,128)(2,1)S(1)}, bf16[640,1024]{1,0:T(8,128)(2,1)}, u32[]{:S(2)}) copy-start(bf16[640,1024]{1,0:T(8,128)(2,1)} %param.6) | copy-start | bytes 3932164
  6.5 85.9 %all-gather.10.cloned.1.call-start = ((), (), s32[]{:S(2)}) async-start(), calls=%async_computation.1 | async-start | bytes 5242880 | tf_op jit(solution)/shard_map/all_gather | solution.py:38
  7.3 125.6 %all-gather.8.cloned.1.call-start = ((), (), s32[]{:S(2)}) async-start(), calls=%async_computation | async-start | bytes 6553600 | tf_op jit(solution)/shard_map/all_gather | solution.py:52
  18.2 2.9 copy-start.1
  19.7 195.6 %all-gather.12.cloned.1.call-start = ((), (), s32[]{:S(2)}) async-start(), calls=%async_computation.2 | async-start | bytes 5242880 | tf_op jit(solution)/shard_map/all_gather | solution.py:39
  20.4 275.5 %all-gather.16.cloned.1.call-start = ((), (), s32[]{:S(2)}) async-start(), calls=%async_computation.4 | async-start | bytes 5242880 | tf_op jit(solution)/shard_map/all_gather | solution.py:40
  21.0 293.1 %all-gather.14.cloned.1.call-start = ((), (), s32[]{:S(2)}) async-start(), calls=%async_computation.3 | async-start | bytes 1638400 | tf_op jit(solution)/shard_map/all_gather | solution.py:81
  137.6 4.7 %collective-permute-start = (bf16[8,256]{1,0:T(8,128)(2,1)S(1)}, bf16[8,256]{1,0:T(8,128)(2,1)S(1)}, u32[]{:S(2)}, u32[]{:S(2)}) collective-permute-start(bf16[8,256]{1,0:T(8,128)(2,1)S(1)} %get-tuple-element.9), channel_id=1, source_target_pairs={{0,4},{4,8},{8,12},{1,5},{5,9},{9,13},{2,6},{6,10},{10,14},{3,7},{... | collective-permute-start | bytes 12296 | tf_op jit(solution)/shard_map/ppermute | solution.py:19
  141.0 5.5 %collective-permute-start.1 = (bf16[8,256]{1,0:T(8,128)(2,1)S(1)}, bf16[8,256]{1,0:T(8,128)(2,1)S(1)}, u32[]{:S(2)}, u32[]{:S(2)}) collective-permute-start(bf16[8,256]{1,0:T(8,128)(2,1)S(1)} %get-tuple-element.10), channel_id=1, source_target_pairs={{4,0},{8,4},{12,8},{5,1},{9,5},{13,9},{6,2},{10,6},{14,10},{7,3},{... | collective-permute-start | bytes 12296 | tf_op jit(solution)/shard_map/ppermute | solution.py:20
  220.7 146.1 %all-gather.18.cloned.1.call-start = ((), (), s32[]{:S(2)}) async-start(), calls=%async_computation.5 | async-start | bytes 6553600 | tf_op jit(solution)/shard_map/all_gather | solution.py:52
  325.2 80.5 %all-gather.20.cloned.1.call-start = ((), (), s32[]{:S(2)}) async-start(), calls=%async_computation.6 | async-start | bytes 1638400 | tf_op jit(solution)/shard_map/all_gather | solution.py:81
  371.5 4.9 %collective-permute-start.2 = (bf16[8,256]{1,0:T(8,128)(2,1)S(1)}, bf16[8,256]{1,0:T(8,128)(2,1)S(1)}, u32[]{:S(2)}, u32[]{:S(2)}) collective-permute-start(bf16[8,256]{1,0:T(8,128)(2,1)S(1)} %get-tuple-element.7), channel_id=1, source_target_pairs={{0,4},{4,8},{8,12},{1,5},{5,9},{9,13},{2,6},{6,10},{10,14},{3,7},{... | collective-permute-start | bytes 12296 | tf_op jit(solution)/shard_map/ppermute | solution.py:19
  374.9 5.5 %collective-permute-start.3 = (bf16[8,256]{1,0:T(8,128)(2,1)S(1)}, bf16[8,256]{1,0:T(8,128)(2,1)S(1)}, u32[]{:S(2)}, u32[]{:S(2)}) collective-permute-start(bf16[8,256]{1,0:T(8,128)(2,1)S(1)} %get-tuple-element.8), channel_id=1, source_target_pairs={{4,0},{8,4},{12,8},{5,1},{9,5},{13,9},{6,2},{10,6},{14,10},{7,3},{... | collective-permute-start | bytes 12296 | tf_op jit(solution)/shard_map/ppermute | solution.py:20
Sparse Core Ops, SparseCore 0:
  8.9 83.4 all-gather.9
  94.0 38.8 all-gather.7
  134.5 80.7 all-gather.11
  216.7 79.1 all-gather.15
  297.3 16.7 all-gather.13
  325.3 41.4 all-gather.17
  388.2 17.3 all-gather.19
where the time goes:
time: 417 us
  waiting for transfers between devices  341 us (82%)
  matrix products  29 us (7%)
  blocking collectives  14.3 us (3%)
  between operations  13.7 us (3%)
  starting transfers between devices  9.78 us (2%)
  other arithmetic  7.59 us (2%)
    all_gather x2, waiting for transfers between devices, local(): piece = lax.all_gather(normed, 'tp', axis=1, tiled=True)  82.1 us
    all_gather x1, waiting for transfers between devices, local(): lax.all_gather(w_out, 'sp', axis=1, tiled=True)  75.1 us
    all_gather x1, waiting for transfers between devices, local(): lax.all_gather(w_pool_in, 'sp', axis=1, tiled=True)  71.2 us
    all_gather x1, waiting for transfers between devices, local(): lax.all_gather(w_pool_gate, 'sp', axis=1, tiled=True)  66.5 us
    all_gather x2, waiting for transfers between devices, local(): lax.all_gather(branch, 'tp', axis=1, tiled=True)  35.8 us
    psum x2, blocking collectives, local(): squares = lax.psum(jnp.sum(resid_f * resid_f, axis=1), 'tp')  14.3 us
    dot_general x2, matrix products, local(): gate_sum = jnp.dot(piece, weight_gate, preferred_element_type=jnp.float32)  10.9 us
    dot_general x2, matrix products, local(): pool_sum = jnp.dot(piece, weight_in, preferred_element_type=jnp.float32)  9.35 us
  transfers between devices with their start and end apart: 11, of which 9 were waited for; matrix products, arithmetic and copies ran while one was open for 4% of the time, Pallas kernels for 0%

commit v1 on v0

v1 whole, which is shorter than its diff:
```python
import functools

import jax
import jax.numpy as jnp
from jax import lax
from jax.experimental import pallas as pl
from jax.experimental.pallas import tpu as pltpu
from jax.sharding import PartitionSpec as P

GROUP = 64
HALO = 8
MESH = pl.DeviceIdType.MESH

norm_eps = 1e-06


def mixer(dims, h_in, gain, w_in, w_gate, mix, w_out, out, hg, nb, br, wi, wg, wo, pad, acc_p, acc_g, bd,
          local_sem, zr, zs, yr, ys, gr, gs, pr, ps):
    sp_size, tp_size, layers, rows, cols, chans, chunks = dims
    step_rows = rows // chunks
    chips = tp_size // 2
    half = lax.axis_index("grp")
    row_rank = lax.axis_index("sp")
    rank = lax.axis_index("tp")
    chip, core = rank // 2, lax.rem(rank, 2)
    sibling = chip * 2 + 1 - core
    other = 1 - half
    total_rows = rows * sp_size
    shards = ((w_in, wi), (w_gate, wg), (w_out, wo))

    def chip_rank(distance):
        return lax.rem(chip + distance, chips) * 2 + core

    own_h = pltpu.make_async_copy(h_in, hg.at[0, rank], local_sem.at[0])
    own_h.start()
    own_w = []
    for layer in range(layers):
        for t, (shard, whole) in enumerate(shards):
            depth = shard.shape[1]
            copy = pltpu.make_async_copy(
                shard.at[layer],
                whole.at[layer, pl.ds(pl.multiple_of(row_rank * depth, depth), depth)],
                local_sem.at[1 + layer * 3 + t],
            )
            copy.start()
            own_w.append(copy)

    barrier = pltpu.get_barrier_semaphore()
    peers = [
        {"sp": lax.rem(row_rank + 1, sp_size)},
        {"sp": lax.rem(row_rank + sp_size - 1, sp_size)},
        {"grp": other},
        {"tp": sibling},
    ] + [{"tp": chip_rank(d)} for d in range(1, chips)]
    for peer in peers:
        pl.semaphore_signal(barrier, inc=1, device_id=peer, device_id_type=MESH)
    pl.semaphore_wait(barrier, len(peers))

    def z_copy(layer, t, source, part, to, send):
        shard, whole = shards[t]
        depth = shard.shape[1]
        piece = depth // 2
        start = pl.multiple_of(source * depth + part * piece, piece)
        ref = whole.at[layer, pl.ds(start, piece)]
        return pltpu.make_async_remote_copy(
            ref, ref, zs.at[layer * 3 + t, send], zr.at[layer * 3 + t, source],
            device_id={"sp": to}, device_id_type=MESH,
        )

    def y_copy(layer, t, source, part):
        shard, whole = shards[t]
        depth = shard.shape[1]
        piece = depth // 2
        start = pl.multiple_of(source * depth + part * piece, piece)
        ref = whole.at[layer, pl.ds(start, piece)]
        return pltpu.make_async_remote_copy(
            ref, ref, ys.at[layer * 3 + t, source], yr.at[layer * 3 + t, source],
            device_id={"grp": other}, device_id_type=MESH,
        )

    up = jnp.minimum(row_rank + 1, sp_size - 1)
    down = jnp.maximum(row_rank - 1, 0)

    def z_own(layer):
        for t in range(3):
            @pl.when(row_rank < sp_size - 1)
            def _():
                z_copy(layer, t, row_rank, half, up, row_rank).start()

            @pl.when(row_rank > 0)
            def _():
                z_copy(layer, t, row_rank, half, down, sp_size).start()

    def z_step(layer, distance, t):
        low, high = row_rank - distance, row_rank + distance

        @pl.when(low >= 0)
        def _():
            z_copy(layer, t, low, half, up, low).wait_recv()

            @pl.when(row_rank < sp_size - 1)
            def _():
                z_copy(layer, t, low, half, up, low).start()

            y_copy(layer, t, low, half).start()

        @pl.when(high < sp_size)
        def _():
            z_copy(layer, t, high, half, down, high).wait_recv()

            @pl.when(row_rank > 0)
            def _():
                z_copy(layer, t, high, half, down, high).start()

            y_copy(layer, t, high, half).start()

    def y_arrived(layer, t):
        for source in range(sp_size):
            @pl.when(row_rank != source)
            def _():
                y_copy(layer, t, source, other).wait_recv()

    def weights_sent():
        for layer in range(layers):
            for t in range(3):
                for source in range(sp_size):
                    @pl.when(row_rank != source)
                    def _():
                        y_copy(layer, t, source, half).wait_send()

                    @pl.when((source <= row_rank) & (row_rank < sp_size - 1))
                    def _():
                        z_copy(layer, t, source, half, up, source).wait_send()

                    @pl.when((source > row_rank) & (row_rank > 0))
                    def _():
                        z_copy(layer, t, source, half, down, source).wait_send()

                @pl.when(row_rank > 0)
                def _():
                    z_copy(layer, t, row_rank, half, down, sp_size).wait_send()

    def g_copy(kind, layer, chunk, source, to, send):
        buffer = (hg, br)[kind]
        ref = buffer.at[layer, source, pl.ds(chunk * step_rows, step_rows)]
        index = (kind * layers + layer) * chunks + chunk
        return pltpu.make_async_remote_copy(
            ref, ref, gs.at[index, send], gr.at[index, source], device_id={"tp": to}, device_id_type=MESH
        )

    def g_send(kind, layer, chunk):
        for d in range(1, chips):
            g_copy(kind, layer, chunk, rank, chip_rank(d), d).start()
        g_copy(kind, layer, chunk, rank, sibling, 0).start()

    def g_relay(kind, layer, chunk):
        for d in range(1, chips):
            source = chip_rank(d)
            g_copy(kind, layer, chunk, source, sibling, chips + d - 1).wait_recv()
            g_copy(kind, layer, chunk, source, sibling, chips + d - 1).start()

    def g_arrived(kind, layer, chunk):
        for d in range(chips):
            source = lax.rem(chip + d, chips) * 2 + 1 - core
            g_copy(kind, layer, chunk, source, sibling, 0).wait_recv()

    def g_sent(kind, layer, chunk):
        for d in range(1, chips):
            g_copy(kind, layer, chunk, rank, chip_rank(d), d).wait_send()
            g_copy(kind, layer, chunk, chip_rank(d), sibling, chips + d - 1).wait_send()
        g_copy(kind, layer, chunk, rank, sibling, 0).wait_send()

    def normalize(layer, chunk):
        span = pl.ds(chunk * step_rows, step_rows)
        squares = jnp.zeros((step_rows, 1), jnp.float32)
        for k in range(tp_size):
            block = hg[layer, k, span, :].astype(jnp.float32)
            squares = squares + jnp.sum(block * block, axis=1, keepdims=True)
        scaling = lax.rsqrt(squares / (cols * tp_size) + norm_eps)
        for k in range(tp_size):
            block = hg[layer, k, span, :].astype(jnp.float32)
            own_gain = gain[layer : layer + 1, k * cols : (k + 1) * cols]
            nb[k, span, :] = (block * scaling * own_gain).astype(jnp.bfloat16)

    def project(acc, whole, layer):
        acc[...] = jnp.zeros_like(acc)

        @pl.loop(0, tp_size)
        def _(k):
            weight = whole[layer, pl.ds(pl.multiple_of(k * cols, cols), cols), :]
            acc[...] += jnp.dot(nb[k], weight, preferred_element_type=jnp.float32)

    def halo_copy(layer, upward):
        source, target = (rows, 0) if upward else (HALO, rows + HALO)
        side = 0 if upward else 1
        return pltpu.make_async_remote_copy(
            pad.at[layer, pl.ds(source, HALO)], pad.at[layer, pl.ds(target, HALO)],
            ps.at[layer, side], pr.at[layer, side],
            device_id={"sp": up if upward else down}, device_id_type=MESH,
        )

    def halo_send(layer):
        @pl.when(row_rank < sp_size - 1)
        def _():
            halo_copy(layer, True).start()

        @pl.when(row_rank > 0)
        def _():
            halo_copy(layer, False).start()

    def halo_arrived(layer):
        @pl.when(row_rank > 0)
        def _():
            halo_copy(layer, True).wait_recv()

        @pl.when(row_rank < sp_size - 1)
        def _():
            halo_copy(layer, False).wait_recv()

    def halo_sent(layer):
        @pl.when(row_rank < sp_size - 1)
        def _():
            halo_copy(layer, True).wait_send()

        @pl.when(row_rank > 0)
        def _():
            halo_copy(layer, False).wait_send()

    groups = chans // GROUP

    def mix_matrix(layer):
        for g in range(groups):
            block = mix[layer, rank * groups + g].astype(jnp.float32)
            parts = [block if g == c else jnp.zeros((GROUP, GROUP), jnp.float32) for c in range(groups)]
            wide = parts[0] if groups == 1 else jnp.concatenate(parts, axis=1)
            bd[layer, g * GROUP : (g + 1) * GROUP, :] = wide.astype(jnp.bfloat16)

    def pool_chunk(layer, chunk):
        base = chunk * step_rows
        length = step_rows + 2 * HALO
        x = pad[layer, base : base + length, :]

        def ahead(v, n):
            return pltpu.roll(v, length - n, 0)

        sum1 = x + ahead(x, 1)
        sum2 = sum1 + ahead(sum1, 2)
        sum4 = sum2 + ahead(sum2, 4)
        sum8 = sum4 + ahead(sum4, 8)
        lane = lax.broadcasted_iota(jnp.int32, (step_rows, chans), 1)
        code = lax.rem(rank * groups + lane // GROUP, 4)
        position = row_rank * rows + base + lax.broadcasted_iota(jnp.int32, (step_rows, chans), 0)
        running = jnp.where(
            code == 0, ahead(sum1, 7)[:step_rows],
            jnp.where(
                code == 1, ahead(sum2, 6)[:step_rows],
                jnp.where(code == 2, ahead(sum4, 4)[:step_rows], sum8[:step_rows]),
            ),
        )
        window = jnp.where(code == 0, 1, jnp.where(code == 1, 2, jnp.where(code == 2, 4, 8)))
        counted = (jnp.minimum(position + window, total_rows) - jnp.maximum(position - window, 0)).astype(jnp.float32)
        pooled = (running / counted - x[HALO : HALO + step_rows]).astype(jnp.bfloat16)
        mixed = jnp.dot(pooled, bd[layer], preferred_element_type=jnp.float32)
        gate = acc_g[base : base + step_rows, :].astype(jnp.bfloat16).astype(jnp.float32)
        branch = mixed * (gate / (1.0 + jnp.exp(-gate)))
        br[layer, rank, pl.ds(base, step_rows), :] = branch.astype(jnp.bfloat16)

    def out_chunk(layer, chunk):
        span = pl.ds(chunk * step_rows, step_rows)
        total = hg[layer, rank, span, :].astype(jnp.float32)
        for k in range(tp_size):
            total = total + jnp.dot(
                br[layer, k, span, :], wo[layer, k * chans : (k + 1) * chans, :],
                preferred_element_type=jnp.float32,
            )
        if layer + 1 < layers:
            hg[layer + 1, rank, span, :] = total.astype(jnp.bfloat16)
        else:
            out[span, :] = total.astype(jnp.bfloat16)

    own_h.wait()
    for chunk in range(chunks):
        g_send(0, 0, chunk)
    for copy in own_w:
        copy.wait()
    z_own(0)
    for layer in range(layers):
        mix_matrix(layer)
        for row in (0, rows + HALO):
            @pl.when(row_rank == (0 if row == 0 else sp_size - 1))
            def _():
                pad[layer, row : row + HALO, :] = jnp.zeros((HALO, chans), jnp.float32)

    gather_tasks = [functools.partial(g_relay, 0, 0, chunk) for chunk in range(chunks)]
    weight_tasks = [functools.partial(z_step, 0, d, t) for d in range(1, sp_size) for t in range(3)]

    for layer in range(layers):
        last = layer + 1 == layers
        done = 0
        pairs = max(len(gather_tasks), len(weight_tasks))
        for turn in range(pairs):
            if turn < len(gather_tasks):
                gather_tasks[turn]()
            if turn < len(weight_tasks):
                weight_tasks[turn]()
            if 1 <= turn <= chunks:
                g_arrived(0, layer, turn - 1)
                normalize(layer, turn - 1)
                done = turn
        for chunk in range(done, chunks):
            g_arrived(0, layer, chunk)
            normalize(layer, chunk)
        if not last:
            z_own(layer + 1)
        later = [] if last else [functools.partial(z_step, layer + 1, d, t) for d in range(1, sp_size) for t in range(3)]
        y_arrived(layer, 0)
        project(acc_p, wi, layer)
        pad[layer, HALO : HALO + rows, :] = acc_p[...].astype(jnp.bfloat16).astype(jnp.float32)
        halo_send(layer)
        y_arrived(layer, 1)
        project(acc_g, wg, layer)
        halo_arrived(layer)
        for chunk in range(chunks):
            pool_chunk(layer, chunk)
            g_send(1, layer, chunk)
        for task in later[:1]:
            task()
        for chunk in range(chunks):
            g_relay(1, layer, chunk)
        y_arrived(layer, 2)
        for chunk in range(chunks):
            g_arrived(1, layer, chunk)
            out_chunk(layer, chunk)
            if not last:
                g_send(0, layer + 1, chunk)
        for task in later[1:3]:
            task()
        weight_tasks = later[3:]
        gather_tasks = [] if last else [functools.partial(g_relay, 0, layer + 1, chunk) for chunk in range(chunks)]

    weights_sent()
    for layer in range(layers):
        halo_sent(layer)
        for kind in range(2):
            for chunk in range(chunks):
                g_sent(kind, layer, chunk)


def solution(mesh):
    sp_size, tp_size = mesh.shape["sp"], mesh.shape["tp"]

    def local(hidden_in, norm_gain, w_pool_in, w_pool_gate, group_mix, w_out):
        rows, cols = hidden_in.shape
        layers, _, chans = w_pool_in.shape
        width, channels = cols * tp_size, chans * tp_size
        chunks = rows // 128 if tp_size <= 4 else 1
        dims = (sp_size, tp_size, layers, rows, cols, chans, chunks)
        bf16, f32 = jnp.bfloat16, jnp.float32
        dma = pltpu.SemaphoreType.DMA
        hbm, vmem = pl.BlockSpec(memory_space=pl.ANY), pl.BlockSpec(memory_space=pltpu.VMEM)
        return pl.pallas_call(
            functools.partial(mixer, dims),
            out_shape=jax.ShapeDtypeStruct((rows, cols), bf16),
            in_specs=[hbm, vmem, hbm, hbm, vmem, hbm],
            out_specs=vmem,
            scratch_shapes=[
                pltpu.VMEM((layers, tp_size, rows, cols), bf16),
                pltpu.VMEM((tp_size, rows, cols), bf16),
                pltpu.VMEM((layers, tp_size, rows, chans), bf16),
                pltpu.VMEM((layers, width, chans), bf16),
                pltpu.VMEM((layers, width, chans), bf16),
                pltpu.VMEM((layers, channels, cols), bf16),
                pltpu.VMEM((layers, rows + 2 * HALO, chans), f32),
                pltpu.VMEM((rows, chans), f32),
                pltpu.VMEM((rows, chans), f32),
                pltpu.VMEM((layers, chans, chans), bf16),
                dma((1 + 3 * layers,)),
                dma((3 * layers, sp_size)),
                dma((3 * layers, sp_size + 1)),
                dma((3 * layers, sp_size)),
                dma((3 * layers, sp_size)),
                dma((2 * layers * chunks, tp_size)),
                dma((2 * layers * chunks, tp_size)),
                dma((layers, 2)),
                dma((layers, 2)),
            ],
            compiler_params=pltpu.CompilerParams(
                collective_id=0, has_side_effects=True, vmem_limit_bytes=60 * 1024 * 1024
            ),
        )(hidden_in, norm_gain, w_pool_in, w_pool_gate, group_mix, w_out)

    in_specs = (
        P(("grp", "sp"), "tp"),
        P(),
        P(None, "sp", "tp"),
        P(None, "sp", "tp"),
        P(),
        P(None, "sp", "tp"),
    )
    out_specs = P(("grp", "sp"), "tp")
    return jax.shard_map(local, mesh=mesh, in_specs=in_specs, out_specs=out_specs, check_vma=False)
```

time: 417 us -> 145 us (0.35)
  waiting for transfers between devices: 341 us -> 0 us
  Pallas kernels: 0 us -> 143 us
  matrix products: 29 us -> 0 us
  blocking collectives: 14.3 us -> 0 us
  between operations: 13.7 us -> 0.01 us
  starting transfers between devices: 9.78 us -> 0 us
  other arithmetic: 7.59 us -> 0 us
    all_gather x7 -> x0, waiting for transfers between devices: 331 us -> none  [the longest x2 82.1 us: local(): piece = lax.all_gather(normed, 'tp', axis=1, tiled=True)]
    pallas_call x0 -> x1, Pallas kernels: none -> 143 us  [local(): pl.pallas_call(functools.partial(mixer, dims), out_shape=jax.ShapeDtypeSt...]
    dot_general x8 -> x0, matrix products: 29 us -> none  [the longest x2 10.9 us: local(): gate_sum = jnp.dot(piece, weight_gate, preferred_element_type=jnp.float32)]
    psum x2 -> x0, blocking collectives: 14.3 us -> none  [local(): squares = lax.psum(jnp.sum(resid_f * resid_f, axis=1), 'tp')]
    ppermute x4 -> x0, starting transfers between devices: 9.54 us -> none  [the longest x2 6.78 us: with_halo(): before = lax.ppermute(last, axis, up)]
    ppermute x4 -> x0, waiting for transfers between devices: 8.19 us -> none  [the longest x2 8.19 us: with_halo(): after = lax.ppermute(leading, axis, down)]
    convert_element_type x8 -> x0, other arithmetic: 5.9 us -> none  [the longest x2 2.93 us: local(): pooled = (averaged - padded[8:8 + tok_rows]).astype(jnp.bfloat16)]
  transfers between devices with their start and end apart: 11 -> 0, of which waited for: 9 -> 0; matrix products, arithmetic and copies ran while one was open for 4% -> 0% of each run, Pallas kernels for 0% -> 0%
where the time goes in v1:
time: 145 us
  Pallas kernels  143 us (99%)
  local copies, waits for them, and re-layouts  2.47 us (2%)
    pallas_call x1, Pallas kernels, local(): pl.pallas_call(functools.partial(mixer, dims), out_shape=jax.ShapeDtypeSt...  143 us

profile of v1, /device:TPU:0, one launch (start us, length us, event | category | flops | bytes accessed | tf_op | source)
XLA Modules:
  0.0 145.0 jit_solution(9753799353505947906)
XLA Ops:
  0.0 142.6 %shard_map.64 = bf16[640,1024]{1,0:T(8,128)(2,1)} custom-call(bf16[640,1024]{1,0:T(8,128)(2,1)} %h_in.1, f32[2,4096]{1,0:T(2,128)} %gain.1, bf16[2,1024,256]{2,1,0:T(8,128)(2,1)} %w_in.1, bf16[2,1024,256]{2,1,0:T(8,128)(2,1)} %w_gate.1, bf16[2,16,64,64]{3,2,1,0:T(8,128)(2,1)} %mix.1, bf16[2,256,1024]{2,1,0:T(8,128)(2,1)} %w_out.1), custom_call_target="tpu_custom_call" | custom-call | tf_op jit(solution)/shard_map/pallas_call | solution.py:361
  142.6 2.5 %copy.8 = bf16[640,1024]{1,0:T(8,128)(2,1)} copy(bf16[640,1024]{1,0:T(8,128)(2,1)} %shard_map.64) | data formatting | bytes 2621440

commit v2 on v1

--- a/solution.py
+++ b/solution.py
@@ -9,6 +9,11 @@
 
 GROUP = 64
 HALO = 8
+SUBS = 1
+AHEAD = 2
+START = (0.0, 0.23)
+GATHERED = (0.56, 0.78)
+POOLED = 0.9
 MESH = pl.DeviceIdType.MESH
 
 norm_eps = 1e-06
@@ -56,89 +61,103 @@
         pl.semaphore_signal(barrier, inc=1, device_id=peer, device_id_type=MESH)
     pl.semaphore_wait(barrier, len(peers))
 
-    def z_copy(layer, t, source, part, to, send):
+    pieces = [(layer, t, sub) for layer in range(layers) for t in range(3) for sub in range(SUBS)]
+
+    def piece_ref(q, source, part):
+        layer, t, sub = pieces[q]
         shard, whole = shards[t]
         depth = shard.shape[1]
-        piece = depth // 2
-        start = pl.multiple_of(source * depth + part * piece, piece)
-        ref = whole.at[layer, pl.ds(start, piece)]
+        size = depth // (2 * SUBS)
+        start = pl.multiple_of(source * depth + (part * SUBS + sub) * size, size)
+        return whole.at[layer, pl.ds(start, size)]
+
+    def z_copy(q, source, to, send):
+        ref = piece_ref(q, source, half)
         return pltpu.make_async_remote_copy(
-            ref, ref, zs.at[layer * 3 + t, send], zr.at[layer * 3 + t, source],
-            device_id={"sp": to}, device_id_type=MESH,
+            ref, ref, zs.at[q, send], zr.at[q, source], device_id={"sp": to}, device_id_type=MESH
         )
 
-    def y_copy(layer, t, source, part):
-        shard, whole = shards[t]
-        depth = shard.shape[1]
-        piece = depth // 2
-        start = pl.multiple_of(source * depth + part * piece, piece)
-        ref = whole.at[layer, pl.ds(start, piece)]
+    def y_copy(q, source, part):
+        ref = piece_ref(q, source, part)
         return pltpu.make_async_remote_copy(
-            ref, ref, ys.at[layer * 3 + t, source], yr.at[layer * 3 + t, source],
-            device_id={"grp": other}, device_id_type=MESH,
+            ref, ref, ys.at[q, source], yr.at[q, source], device_id={"grp": other}, device_id_type=MESH
         )
 
     up = jnp.minimum(row_rank + 1, sp_size - 1)
     down = jnp.maximum(row_rank - 1, 0)
 
-    def z_own(layer):
-        for t in range(3):
+    def z_own(q):
+        layer, t, sub = pieces[q]
+        if sub == 0:
+            own_w[layer * 3 + t].wait()
+
+        @pl.when(row_rank < sp_size - 1)
+        def _():
+            z_copy(q, row_rank, up, row_rank).start()
+
+        @pl.when(row_rank > 0)
+        def _():
+            z_copy(q, row_rank, down, sp_size).start()
+
+    def z_step(q, distance):
+        low, high = row_rank - distance, row_rank + distance
+
+        @pl.when(low >= 0)
+        def _():
+            z_copy(q, low, up, low).wait_recv()
+
             @pl.when(row_rank < sp_size - 1)
             def _():
-                z_copy(layer, t, row_rank, half, up, row_rank).start()
+                z_copy(q, low, up, low).start()
+
+            y_copy(q, low, half).start()
+
+        @pl.when(high < sp_size)
+        def _():
+            z_copy(q, high, down, high).wait_recv()
 
             @pl.when(row_rank > 0)
             def _():
-                z_copy(layer, t, row_rank, half, down, sp_size).start()
-
-    def z_step(layer, distance, t):
-        low, high = row_rank - distance, row_rank + distance
-
-        @pl.when(low >= 0)
-        def _():
-            z_copy(layer, t, low, half, up, low).wait_recv()
-
-            @pl.when(row_rank < sp_size - 1)
-            def _():
-                z_copy(layer, t, low, half, up, low).start()
-
-            y_copy(layer, t, low, half).start()
-
-        @pl.when(high < sp_size)
-        def _():
-            z_copy(layer, t, high, half, down, high).wait_recv()
-
-            @pl.when(row_rank > 0)
-            def _():
-                z_copy(layer, t, high, half, down, high).start()
-
-            y_copy(layer, t, high, half).start()
+                z_copy(q, high, down, high).start()
+
+            y_copy(q, high, half).start()
+
+        if distance == sp_size - 1 and q + AHEAD < len(pieces):
+            z_own(q + AHEAD)
+
+    steps = [functools.partial(z_step, q, d) for q in range(len(pieces)) for d in range(1, sp_size)]
+
+    def advance(upto):
+        while steps and len(pieces) * (sp_size - 1) - len(steps) < upto:
+            steps.pop(0)()
 
     def y_arrived(layer, t):
-        for source in range(sp_size):
-            @pl.when(row_rank != source)
-            def _():
-                y_copy(layer, t, source, other).wait_recv()
-
-    def weights_sent():
-        for layer in range(layers):
-            for t in range(3):
+        for q, piece in enumerate(pieces):
+            if piece[:2] == (layer, t):
+                advance((q + 1) * (sp_size - 1))
                 for source in range(sp_size):
                     @pl.when(row_rank != source)
                     def _():
-                        y_copy(layer, t, source, half).wait_send()
-
-                    @pl.when((source <= row_rank) & (row_rank < sp_size - 1))
-                    def _():
-                        z_copy(layer, t, source, half, up, source).wait_send()
-
-                    @pl.when((source > row_rank) & (row_rank > 0))
-                    def _():
-                        z_copy(layer, t, source, half, down, source).wait_send()
-
-                @pl.when(row_rank > 0)
+                        y_copy(q, source, other).wait_recv()
+
+    def weights_sent():
+        for q in range(len(pieces)):
+            for source in range(sp_size):
+                @pl.when(row_rank != source)
                 def _():
-                    z_copy(layer, t, row_rank, half, down, sp_size).wait_send()
+                    y_copy(q, source, half).wait_send()
+
+                @pl.when((source <= row_rank) & (row_rank < sp_size - 1))
+                def _():
+                    z_copy(q, source, up, source).wait_send()
+
+                @pl.when((source > row_rank) & (row_rank > 0))
+                def _():
+                    z_copy(q, source, down, source).wait_send()
+
+            @pl.when(row_rank > 0)
+            def _():
+                z_copy(q, row_rank, down, sp_size).wait_send()
 
     def g_copy(kind, layer, chunk, source, to, send):
         buffer = (hg, br)[kind]
@@ -281,9 +300,8 @@
     own_h.wait()
     for chunk in range(chunks):
         g_send(0, 0, chunk)
-    for copy in own_w:
-        copy.wait()
-    z_own(0)
+    for q in range(AHEAD):
+        z_own(q)
     for layer in range(layers):
         mix_matrix(layer)
         for row in (0, rows + HALO):
@@ -291,28 +309,21 @@
             def _():
                 pad[layer, row : row + HALO, :] = jnp.zeros((HALO, chans), jnp.float32)
 
-    gather_tasks = [functools.partial(g_relay, 0, 0, chunk) for chunk in range(chunks)]
-    weight_tasks = [functools.partial(z_step, 0, d, t) for d in range(1, sp_size) for t in range(3)]
+    per_layer = len(pieces) // layers * (sp_size - 1)
+
+    def pace(layer, part):
+        advance(layer * per_layer + int(per_layer * part))
 
     for layer in range(layers):
         last = layer + 1 == layers
-        done = 0
-        pairs = max(len(gather_tasks), len(weight_tasks))
-        for turn in range(pairs):
-            if turn < len(gather_tasks):
-                gather_tasks[turn]()
-            if turn < len(weight_tasks):
-                weight_tasks[turn]()
-            if 1 <= turn <= chunks:
-                g_arrived(0, layer, turn - 1)
-                normalize(layer, turn - 1)
-                done = turn
-        for chunk in range(done, chunks):
-            g_arrived(0, layer, chunk)
-            normalize(layer, chunk)
-        if not last:
-            z_own(layer + 1)
-        later = [] if last else [functools.partial(z_step, layer + 1, d, t) for d in range(1, sp_size) for t in range(3)]
+        for chunk in range(chunks):
+            g_relay(0, layer, chunk)
+            pace(layer, START[layer > 0] + (GATHERED[layer > 0] - START[layer > 0]) * (chunk + 1) / chunks)
+            if chunk:
+                g_arrived(0, layer, chunk - 1)
+                normalize(layer, chunk - 1)
+        g_arrived(0, layer, chunks - 1)
+        normalize(layer, chunks - 1)
         y_arrived(layer, 0)
         project(acc_p, wi, layer)
         pad[layer, HALO : HALO + rows, :] = acc_p[...].astype(jnp.bfloat16).astype(jnp.float32)
@@ -323,8 +334,7 @@
         for chunk in range(chunks):
             pool_chunk(layer, chunk)
             g_send(1, layer, chunk)
-        for task in later[:1]:
-            task()
+        pace(layer, POOLED)
         for chunk in range(chunks):
             g_relay(1, layer, chunk)
         y_arrived(layer, 2)
@@ -333,10 +343,8 @@
             out_chunk(layer, chunk)
             if not last:
                 g_send(0, layer + 1, chunk)
-        for task in later[1:3]:
-            task()
-        weight_tasks = later[3:]
-        gather_tasks = [] if last else [functools.partial(g_relay, 0, layer + 1, chunk) for chunk in range(chunks)]
+        if not last:
+            pace(layer + 1, START[1])
 
     weights_sent()
     for layer in range(layers):
@@ -375,10 +383,10 @@
                 pltpu.VMEM((rows, chans), f32),
                 pltpu.VMEM((layers, chans, chans), bf16),
                 dma((1 + 3 * layers,)),
-                dma((3 * layers, sp_size)),
-                dma((3 * layers, sp_size + 1)),
-                dma((3 * layers, sp_size)),
-                dma((3 * layers, sp_size)),
+                dma((3 * layers * SUBS, sp_size)),
+                dma((3 * layers * SUBS, sp_size + 1)),
+                dma((3 * layers * SUBS, sp_size)),
+                dma((3 * layers * SUBS, sp_size)),
                 dma((2 * layers * chunks, tp_size)),
                 dma((2 * layers * chunks, tp_size)),
                 dma((layers, 2)),

time: 145 us -> 135 us (0.931)
  Pallas kernels: 143 us -> 132 us
    pallas_call x1, Pallas kernels: 143 us -> 132 us  [local(): pl.pallas_call(functools.partial(mixer, dims), out_shape=jax.ShapeDtypeSt...]
where the time goes in v2:
time: 135 us
  Pallas kernels  132 us (98%)
  local copies, waits for them, and re-layouts  2.47 us (2%)
    pallas_call x1, Pallas kernels, local(): pl.pallas_call(functools.partial(mixer, dims), out_shape=jax.ShapeDtypeSt...  132 us

profile of v2, /device:TPU:0, one launch (start us, length us, event | category | flops | bytes accessed | tf_op | source)
XLA Modules:
  0.0 134.6 jit_solution(8264444320763254026)
XLA Ops:
  0.0 132.1 %shard_map.64 = bf16[640,1024]{1,0:T(8,128)(2,1)} custom-call(bf16[640,1024]{1,0:T(8,128)(2,1)} %h_in.1, f32[2,4096]{1,0:T(2,128)} %gain.1, bf16[2,1024,256]{2,1,0:T(8,128)(2,1)} %w_in.1, bf16[2,1024,256]{2,1,0:T(8,128)(2,1)} %w_gate.1, bf16[2,16,64,64]{3,2,1,0:T(8,128)(2,1)} %mix.1, bf16[2,256,1024]{2,1,0:T(8,128)(2,1)} %w_out.1), custom_call_target="tpu_custom_call" | custom-call | tf_op jit(solution)/shard_map/pallas_call | solution.py:369
  132.2 2.5 %copy.8 = bf16[640,1024]{1,0:T(8,128)(2,1)} copy(bf16[640,1024]{1,0:T(8,128)(2,1)} %shard_map.64) | data formatting | bytes 2621440

commit v3 on v2

--- a/solution.py
+++ b/solution.py
@@ -11,9 +11,12 @@
 HALO = 8
 SUBS = 1
 AHEAD = 2
-START = (0.0, 0.23)
-GATHERED = (0.56, 0.78)
-POOLED = 0.9
+START = (0.0, 0.34)
+GATHERED = (0.56, 0.67)
+PROJECTED = (0.78, 0.89)
+GATED = (0.89, 1.0)
+POOLED = (1.0, 1.23)
+RELAYED = (1.0, 1.23)
 MESH = pl.DeviceIdType.MESH
 
 norm_eps = 1e-06
@@ -36,8 +39,6 @@
     def chip_rank(distance):
         return lax.rem(chip + distance, chips) * 2 + core
 
-    own_h = pltpu.make_async_copy(h_in, hg.at[0, rank], local_sem.at[0])
-    own_h.start()
     own_w = []
     for layer in range(layers):
         for t, (shard, whole) in enumerate(shards):
@@ -49,6 +50,8 @@
             )
             copy.start()
             own_w.append(copy)
+    own_h = pltpu.make_async_copy(h_in, hg.at[0, rank], local_sem.at[0])
+    own_h.start()
 
     barrier = pltpu.get_barrier_semaphore()
     peers = [
@@ -62,6 +65,13 @@
     pl.semaphore_wait(barrier, len(peers))
 
     pieces = [(layer, t, sub) for layer in range(layers) for t in range(3) for sub in range(SUBS)]
+    final = len(pieces) - 1
+    extra = final + 1
+    pieces.append(pieces[final])
+    ends = (0, sp_size - 1)
+
+    def swapped(q, source):
+        return q < final or (q == final and source not in ends)
 
     def piece_ref(q, source, part):
         layer, t, sub = pieces[q]
@@ -72,7 +82,7 @@
         return whole.at[layer, pl.ds(start, size)]
 
     def z_copy(q, source, to, send):
-        ref = piece_ref(q, source, half)
+        ref = piece_ref(q, source, other if q == extra else half)
         return pltpu.make_async_remote_copy(
             ref, ref, zs.at[q, send], zr.at[q, source], device_id={"sp": to}, device_id_type=MESH
         )
@@ -88,21 +98,21 @@
 
     def z_own(q):
         layer, t, sub = pieces[q]
-        if sub == 0:
+        if sub == 0 and q < extra:
             own_w[layer * 3 + t].wait()
 
-        @pl.when(row_rank < sp_size - 1)
+        @pl.when((row_rank == 0) if q == extra else (row_rank < sp_size - 1))
         def _():
             z_copy(q, row_rank, up, row_rank).start()
 
-        @pl.when(row_rank > 0)
+        @pl.when((row_rank == sp_size - 1) if q == extra else (row_rank > 0))
         def _():
             z_copy(q, row_rank, down, sp_size).start()
 
     def z_step(q, distance):
         low, high = row_rank - distance, row_rank + distance
 
-        @pl.when(low >= 0)
+        @pl.when((low == 0) if q == extra else (low >= 0))
         def _():
             z_copy(q, low, up, low).wait_recv()
 
@@ -110,9 +120,14 @@
             def _():
                 z_copy(q, low, up, low).start()
 
-            y_copy(q, low, half).start()
-
-        @pl.when(high < sp_size)
+            if q < final:
+                y_copy(q, low, half).start()
+            elif q == final:
+                @pl.when(low > 0)
+                def _():
+                    y_copy(q, low, half).start()
+
+        @pl.when((high == sp_size - 1) if q == extra else (high < sp_size))
         def _():
             z_copy(q, high, down, high).wait_recv()
 
@@ -120,7 +135,12 @@
             def _():
                 z_copy(q, high, down, high).start()
 
-            y_copy(q, high, half).start()
+            if q < final:
+                y_copy(q, high, half).start()
+            elif q == final:
+                @pl.when(high < sp_size - 1)
+                def _():
+                    y_copy(q, high, half).start()
 
         if distance == sp_size - 1 and q + AHEAD < len(pieces):
             z_own(q + AHEAD)
@@ -136,6 +156,9 @@
             if piece[:2] == (layer, t):
                 advance((q + 1) * (sp_size - 1))
                 for source in range(sp_size):
+                    if not swapped(q, source):
+                        continue
+
                     @pl.when(row_rank != source)
                     def _():
                         y_copy(q, source, other).wait_recv()
@@ -143,19 +166,22 @@
     def weights_sent():
         for q in range(len(pieces)):
             for source in range(sp_size):
-                @pl.when(row_rank != source)
-                def _():
-                    y_copy(q, source, half).wait_send()
-
-                @pl.when((source <= row_rank) & (row_rank < sp_size - 1))
-                def _():
-                    z_copy(q, source, up, source).wait_send()
-
-                @pl.when((source > row_rank) & (row_rank > 0))
-                def _():
-                    z_copy(q, source, down, source).wait_send()
-
-            @pl.when(row_rank > 0)
+                if swapped(q, source):
+                    @pl.when(row_rank != source)
+                    def _():
+                        y_copy(q, source, half).wait_send()
+
+                if q < extra or source == 0:
+                    @pl.when((source <= row_rank) & (row_rank < sp_size - 1))
+                    def _():
+                        z_copy(q, source, up, source).wait_send()
+
+                if q < extra or source == sp_size - 1:
+                    @pl.when((source > row_rank) & (row_rank > 0))
+                    def _():
+                        z_copy(q, source, down, source).wait_send()
+
+            @pl.when((row_rank == sp_size - 1) if q == extra else (row_rank > 0))
             def _():
                 z_copy(q, row_rank, down, sp_size).wait_send()
 
@@ -297,10 +323,11 @@
         else:
             out[span, :] = total.astype(jnp.bfloat16)
 
+    z_own(0)
     own_h.wait()
     for chunk in range(chunks):
         g_send(0, 0, chunk)
-    for q in range(AHEAD):
+    for q in range(1, AHEAD):
         z_own(q)
     for layer in range(layers):
         mix_matrix(layer)
@@ -309,10 +336,10 @@
             def _():
                 pad[layer, row : row + HALO, :] = jnp.zeros((HALO, chans), jnp.float32)
 
-    per_layer = len(pieces) // layers * (sp_size - 1)
+    per_layer = extra // layers * (sp_size - 1)
 
     def pace(layer, part):
-        advance(layer * per_layer + int(per_layer * part))
+        advance(layer * per_layer + int(per_layer * part + 0.1))
 
     for layer in range(layers):
         last = layer + 1 == layers
@@ -328,21 +355,25 @@
         project(acc_p, wi, layer)
         pad[layer, HALO : HALO + rows, :] = acc_p[...].astype(jnp.bfloat16).astype(jnp.float32)
         halo_send(layer)
+        pace(layer, PROJECTED[layer > 0])
         y_arrived(layer, 1)
         project(acc_g, wg, layer)
+        pace(layer, GATED[layer > 0])
         halo_arrived(layer)
         for chunk in range(chunks):
             pool_chunk(layer, chunk)
             g_send(1, layer, chunk)
-        pace(layer, POOLED)
+        pace(layer, POOLED[layer > 0])
         for chunk in range(chunks):
             g_relay(1, layer, chunk)
+        pace(layer, RELAYED[layer > 0])
         y_arrived(layer, 2)
         for chunk in range(chunks):
             g_arrived(1, layer, chunk)
             out_chunk(layer, chunk)
             if not last:
                 g_send(0, layer + 1, chunk)
+                pace(layer + 1, START[1] * chunk / chunks)
         if not last:
             pace(layer + 1, START[1])
 
@@ -383,10 +414,10 @@
                 pltpu.VMEM((rows, chans), f32),
                 pltpu.VMEM((layers, chans, chans), bf16),
                 dma((1 + 3 * layers,)),
-                dma((3 * layers * SUBS, sp_size)),
-                dma((3 * layers * SUBS, sp_size + 1)),
-                dma((3 * layers * SUBS, sp_size)),
-                dma((3 * layers * SUBS, sp_size)),
+                dma((3 * layers * SUBS + 1, sp_size)),
+                dma((3 * layers * SUBS + 1, sp_size + 1)),
+                dma((3 * layers * SUBS + 1, sp_size)),
+                dma((3 * layers * SUBS + 1, sp_size)),
                 dma((2 * layers * chunks, tp_size)),
                 dma((2 * layers * chunks, tp_size)),
                 dma((layers, 2)),

time: 135 us -> 133 us (0.985)
  Pallas kernels: 132 us -> 130 us
    pallas_call x1, Pallas kernels: 132 us -> 130 us  [local(): pl.pallas_call(functools.partial(mixer, dims), out_shape=jax.ShapeDtypeSt...]
where the time goes in v3:
time: 133 us
  Pallas kernels  130 us (98%)
  local copies, waits for them, and re-layouts  2.47 us (2%)
    pallas_call x1, Pallas kernels, local(): pl.pallas_call(functools.partial(mixer, dims), out_shape=jax.ShapeDtypeSt...  130 us

profile of v3, /device:TPU:0, one launch (start us, length us, event | category | flops | bytes accessed | tf_op | source)
XLA Modules:
  0.0 132.6 jit_solution(8173802370792818186)
XLA Ops:
  0.0 130.1 %shard_map.64 = bf16[640,1024]{1,0:T(8,128)(2,1)} custom-call(bf16[640,1024]{1,0:T(8,128)(2,1)} %h_in.1, f32[2,4096]{1,0:T(2,128)} %gain.1, bf16[2,1024,256]{2,1,0:T(8,128)(2,1)} %w_in.1, bf16[2,1024,256]{2,1,0:T(8,128)(2,1)} %w_gate.1, bf16[2,16,64,64]{3,2,1,0:T(8,128)(2,1)} %mix.1, bf16[2,256,1024]{2,1,0:T(8,128)(2,1)} %w_out.1), custom_call_target="tpu_custom_call" | custom-call | tf_op jit(solution)/shard_map/pallas_call | solution.py:400
  130.2 2.5 %copy.8 = bf16[640,1024]{1,0:T(8,128)(2,1)} copy(bf16[640,1024]{1,0:T(8,128)(2,1)} %shard_map.64) | data formatting | bytes 2621440
